TPU v7x, 32 devices: a whole 2x2x4 slice. The times are simulated.
32 devices in a mesh: grp: 2 (over y), kv: 4 (over z), tp: 4 (over x, core).
Axes of the slice: x: 2, y: 2, z: 4, core: 2. Of those that a mesh axis runs over, the one named last changes fastest.
Arguments:
- tokens: bfloat16 [32, 4096], P('grp', 'kv'), parts along dimension 0, may hold values from -40 to 40
- lengths: int32 [32], P(('grp', 'kv')), parts along dimension 0, may hold values from 1 to 6, 40 in all
- conv_state_x: bfloat16 [32, 3, 4096], P(('grp', 'kv'), None, 'tp'), parts along dimension 0, may hold values from -6 to 6
- conv_state_bc: bfloat16 [32, 3, 2, 1024], P(('grp', 'kv'), None, None, 'tp'), parts along dimension 0, may hold values from -6 to 6
- ssm_state: float32 [32, 64, 64, 128], P(('grp', 'kv'), 'tp'), parts along dimension 0, may hold values from -0.6 to 0.6
- norm_gain: bfloat16 [4096], P('kv'), may hold values from 0.099609375 to 1.8984375
- w_gate: bfloat16 [4096, 4096], P('kv', 'tp'), may hold values from -0.09375 to 0.09375
- w_value: bfloat16 [4096, 4096], P('kv', 'tp'), may hold values from -0.09375 to 0.09375
- w_key: bfloat16 [4096, 1024], P('kv', 'tp'), may hold values from -0.09375 to 0.09375
- w_query: bfloat16 [4096, 1024], P('kv', 'tp'), may hold values from -0.09375 to 0.09375
- w_step: bfloat16 [4096, 64], P('kv', 'tp'), may hold values from -0.09375 to 0.09375
- step_bias: float32 [64], P('tp'), may hold values from -2 to 0
- decay_log: float32 [64], P('tp'), may hold values from -2 to 1
- conv_x: bfloat16 [4, 4096], P(None, 'tp'), may hold values from -3 to 3
- conv_bc: bfloat16 [4, 2, 1024], P(None, None, 'tp'), may hold values from -3 to 3
- inner_gain: bfloat16 [4096], P('tp'), may hold values from 0.099609375 to 1.8984375
- w_out: bfloat16 [4096, 4096], P('tp', 'kv'), may hold values from -0.09375 to 0.09375
- mlp_gain: bfloat16 [4096], P('kv'), may hold values from 0.099609375 to 1.8984375
- w_up: bfloat16 [4096, 16384], P('kv', 'tp'), may hold values from -0.09375 to 0.09375
- w_down: bfloat16 [16384, 4096], P('tp', 'kv'), may hold values from -0.046875 to 0.046875
Outputs:
- layer_out: bfloat16 [32, 4096], P('grp', 'kv'), parts along dimension 0
- next_state: float32 [32, 64, 64, 128], P(('grp', 'kv'), 'tp'), parts along dimension 0
There are 2 independent parts, one for each index of `grp`. A program takes and returns all parts, laid end to end along the dimension named above; an argument that names none is the same for every part. Nothing has to cross between parts.
All inputs are finite; a program needn't handle non-finite values. No bound on the sum of `lengths` on one device may be relied on, other than what follows from the above.
Results may differ from a plain program's by a relative error of at most 0.008.
Values may be sent and summed in bfloat16 or wider, within the bound.
A program may use at most 64 MiB of HBM per device.

v0:
```python
import jax
import jax.numpy as jnp
from jax import lax
from jax.sharding import PartitionSpec as P

D = 4096
HEAD_DIM = 64
STATE = 128
CONV_WIDTH = 4
INNER = 4096


epsilon = 1e-06


def causal_conv(state_rows, newest, conv_weights):
    extended = jnp.concatenate([state_rows, newest[:, None]], axis=1)
    conv_sum = extended[:, 0] * conv_weights[0].astype(jnp.float32)
    for offset in range(1, conv_weights.shape[0]):
        conv_sum = conv_sum + extended[:, offset] * conv_weights[offset].astype(jnp.float32)
    return jax.nn.silu(conv_sum)


def product(left, right):
    return jnp.dot(left, right, preferred_element_type=jnp.float32)


def per_device(
    tokens,
    lengths,
    conv_state_x,
    conv_state_bc,
    ssm_state,
    norm_gain,
    w_gate,
    w_value,
    w_key,
    w_query,
    w_step,
    step_bias,
    decay_log,
    conv_x,
    conv_bc,
    inner_gain,
    w_out,
    mlp_gain,
    w_up,
    w_down,
):
    head_count = w_step.shape[1]
    group_count = w_key.shape[1] // STATE
    per_group = head_count // group_count
    widened = tokens.astype(jnp.float32)
    scaled = (widened * norm_gain.astype(jnp.float32)).astype(jnp.bfloat16)
    gate_raw, value_raw, key_raw, query_raw, step_raw, squares = (
        lax.psum_scatter(product(scaled, w_gate), "kv", scatter_dimension=0, tiled=True),
        lax.psum_scatter(product(scaled, w_value), "kv", scatter_dimension=0, tiled=True),
        lax.psum_scatter(product(scaled, w_key), "kv", scatter_dimension=0, tiled=True),
        lax.psum_scatter(product(scaled, w_query), "kv", scatter_dimension=0, tiled=True),
        lax.psum_scatter(product(scaled, w_step), "kv", scatter_dimension=0, tiled=True),
        lax.psum_scatter(jnp.sum(widened * widened, axis=1), "kv", scatter_dimension=0, tiled=True),
    )
    seq_count = gate_raw.shape[0]
    inverse = lax.rsqrt(squares / D + epsilon)[:, None]
    row_live = (
        jnp.arange(CONV_WIDTH - 1, dtype=jnp.int32)[None, :] >= CONV_WIDTH - 1 - lengths[:, None]
    ).astype(jnp.float32)
    live_x = conv_state_x.astype(jnp.float32) * row_live[:, :, None]
    live_bc = conv_state_bc.astype(jnp.float32) * row_live[:, :, None, None]
    mixed_values = causal_conv(live_x, value_raw * inverse, conv_x).reshape(
        seq_count, head_count, HEAD_DIM
    )
    key_query = causal_conv(
        live_bc, jnp.stack([key_raw * inverse, query_raw * inverse], axis=1), conv_bc
    )
    key_heads = jnp.repeat(
        key_query[:, 0].reshape(seq_count, group_count, STATE), per_group, axis=1
    )
    query_heads = jnp.repeat(
        key_query[:, 1].reshape(seq_count, group_count, STATE), per_group, axis=1
    )
    step_size = jax.nn.softplus(step_raw * inverse + step_bias)
    rate_now = -jnp.exp(decay_log) * step_size
    next_state = (
        ssm_state * jnp.exp(rate_now)[:, :, None, None]
        + (step_size[:, :, None] * mixed_values)[:, :, :, None] * key_heads[:, :, None, :]
    )
    mixer_y = jnp.einsum(
        "bhpn,bhn->bhp", next_state, query_heads, precision=lax.Precision.HIGHEST
    ).reshape(seq_count, head_count * HEAD_DIM)
    gated_rows = mixer_y * jax.nn.silu(gate_raw * inverse)
    gated_low = (gated_rows * inner_gain.astype(jnp.float32)).astype(jnp.bfloat16)
    all_low, all_squares = (
        lax.all_gather(gated_low, "kv", axis=0, tiled=True),
        lax.all_gather(
            jnp.sum(gated_rows * gated_rows, axis=1).astype(jnp.bfloat16), "kv", axis=0, tiled=True
        ).astype(jnp.float32),
    )
    out_sum, gated_total = lax.psum((product(all_low, w_out), all_squares), "tp")
    residual = (widened + out_sum * lax.rsqrt(gated_total / INNER + epsilon)[:, None]).astype(
        jnp.bfloat16
    )
    residual_wide = residual.astype(jnp.float32)
    hidden_low = (residual_wide * mlp_gain.astype(jnp.float32)).astype(jnp.bfloat16)
    row_squares = jnp.sum(residual_wide * residual_wide, axis=1)
    up_sum, square_sum = lax.psum((product(hidden_low, w_up), row_squares), "kv")
    activation = jnp.square(
        jax.nn.relu(up_sum * lax.rsqrt(square_sum / D + epsilon)[:, None])
    ).astype(jnp.bfloat16)
    down_sum = lax.psum(product(activation, w_down), "tp")
    layer_out = (residual_wide + down_sum).astype(jnp.bfloat16)
    return (layer_out, next_state)


def solution(mesh):
    return jax.shard_map(
        per_device,
        mesh=mesh,
        in_specs=(
            P("grp", "kv"),
            P(("grp", "kv")),
            P(("grp", "kv"), None, "tp"),
            P(("grp", "kv"), None, None, "tp"),
            P(("grp", "kv"), "tp", None, None),
            P("kv"),
            P("kv", "tp"),
            P("kv", "tp"),
            P("kv", "tp"),
            P("kv", "tp"),
            P("kv", "tp"),
            P("tp"),
            P("tp"),
            P(None, "tp"),
            P(None, None, "tp"),
            P("tp"),
            P("tp", "kv"),
            P("kv"),
            P("kv", "tp"),
            P("tp", "kv"),
        ),
        out_specs=(P("grp", "kv"), P(("grp", "kv"), "tp", None, None)),
        check_vma=False,
    )
```

profile of v0, /device:TPU:0, one launch (start us, length us, event | category | flops | bytes accessed | tf_op | source)
XLA Modules:
  0.0 207.7 jit_solution(14826090005879602014)
XLA Ops:
  7.2 0.8 convert_element_type.73
  8.1 0.7 copy-done
  8.8 1.9 fusion.26
  10.7 1.0 fusion.20
  11.8 0.1 fusion.4
  12.0 0.1 fusion.28
  12.2 0.2 fusion.24
  12.3 0.2 fusion.22
  12.6 0.7 fusion.47
  13.9 21.3 %all-reduce.7 = (f32[16,256]{1,0:T(8,128)S(1)}, f32[16]{0:T(128)S(1)}, f32[16,256]{1,0:T(8,128)S(1)}, f32[16,16]{1,0:T(8,128)S(1)}) all-reduce(f32[16,256]{1,0:T(8,128)S(1)} %fusion.22, f32[16]{0:T(128)S(1)} %fusion.4, f32[16,256]{1,0:T(8,128)S(1)} %fusion.24, ...), channel_id=6, replica_groups=mesh['grp'=2,'kv'=4,'tp'=4] {'kv'}, use_global_device_ids=true, to_apply=%region_5.0.clone | all-reduce | flops 8464 | bytes 67712
  36.3 0.1 multiply_exponential_fusion
  36.4 13.2 %all-reduce.20.cloned.1.call-done = (f32[16,1024]{1,0:T(8,128)}, f32[16,1024]{1,0:T(8,128)}) async-done(((f32[16,1024]{1,0:T(8,128)}, f32[16,1024]{1,0:T(8,128)}), (f32[16,1024]{1,0:T(8,128)}, f32[16,1024]{1,0:T(8,128)})) %all-reduce.20.cloned.1.call-update) | async-done | bytes 131088
  49.5 0.8 divide_multiply_fusion.1
  50.4 0.1 reshape.72
  50.6 2.1 multiply_add_fusion
  52.7 1.3 copy-done.1
  53.9 3.3 %fusion.48 = f32[4,16,1,64]{3,2,1,0:T(1,128)S(1)} fusion(f32[4,16,64,128]{3,2,1,0:T(8,128)S(1)} %multiply_add_fusion, f32[4,16,128,1]{2,3,1,0:T(1,128)S(1)} %bitcast.104), kind=kOutput, calls=%fused_computation.85 | convolution fusion | flops 6291456 | bytes 2146304 | tf_op jit(solution)/shard_map/bhpn,bhn->bhp/dot_general | solution.py:88
  57.3 0.1 reshape.74
  57.4 1.0 multiply_reduce_fusion
  58.3 0.2 dynamic-update-slice
  58.6 10.6 %all-reduce = bf16[16]{0:T(256)(128)(2,1)S(1)} all-reduce(bf16[16]{0:T(256)(128)(2,1)S(1)} %dynamic-update-slice), channel_id=1, replica_groups=mesh['grp'=2,'kv'=4,'tp'=4] {'kv'}, use_global_device_ids=true, to_apply=%add | all-reduce | flops 16 | bytes 64
  69.2 5.7 %psum.36 = f32[16]{0:T(128)S(1)} all-reduce(bf16[16]{0:T(256)(128)(2,1)S(1)} %all-reduce), channel_id=1, replica_groups=mesh['grp'=2,'kv'=4,'tp'=4] {'tp'}, use_global_device_ids=true, to_apply=%region_9.10 | all-reduce | flops 16 | bytes 96 | tf_op jit(solution)/shard_map/psum | solution.py:99
  74.9 13.1 %all-gather = bf16[4,4,1024]{2,1,0:T(4,128)(2,1)S(1)} all-gather(bf16[1,4,1024]{2,1,0:T(4,128)(2,1)S(1)} %fusion.30), channel_id=1, replica_groups=mesh['grp'=2,'kv'=4,'tp'=4] {'kv'}, dimensions={0}, use_global_device_ids=true | all-gather | bytes 40960 | tf_op jit(solution)/shard_map/all_gather | solution.py:94
  88.0 2.6 %fusion.49 = f32[16,1024]{1,0:T(8,128)} fusion(bf16[16,1024]{1,0:T(8,128)(2,1)S(1)} %reshape.87, bf16[1024,1024]{1,0:T(8,128)(2,1)} %param.36), kind=kOutput, calls=%fused_computation.86 | convolution fusion | flops 33554432 | bytes 2195456 | tf_op jit(solution)/shard_map/dot_general | solution.py:25
  90.7 30.0 %all-reduce.14.cloned.1.call-done = f32[16,1024]{1,0:T(8,128)} async-done(((f32[16,1024]{1,0:T(8,128)}), f32[16,1024]{1,0:T(8,128)}) %all-reduce.14.cloned.1.call-update) | async-done | bytes 65552 | tf_op jit(solution)/shard_map/psum | solution.py:99
  120.7 1.0 fusion.7
  121.7 5.3 %fusion.9 = f32[16,4096]{1,0:T(8,128)} fusion(bf16[1024,4096]{1,0:T(8,128)(2,1)} %param.38, bf16[16,1024]{1,0:T(8,128)(2,1)S(1)} %get-tuple-element.9, f32[1024]{0:T(1024)S(1)} %convert_element_type.84), kind=kOutput, calls=%fused_computation.18 | convolution fusion | flops 134266880 | bytes 8687616 | tf_op jit(solution)/shard_map/dot_general | solution.py:25
  127.1 11.8 %psum.38 = f32[16]{0:T(128)S(1)} all-reduce(f32[16]{0:T(128)S(1)} %get-tuple-element.8), channel_id=1, replica_groups=mesh['grp'=2,'kv'=4,'tp'=4] {'kv'}, use_global_device_ids=true, to_apply=%region_12.13 | all-reduce | flops 16 | bytes 128 | tf_op jit(solution)/shard_map/psum | solution.py:106
  138.9 23.9 %all-reduce.16.cloned.1.call-done = f32[16,4096]{1,0:T(8,128)} async-done(((f32[16,4096]{1,0:T(8,128)}), f32[16,4096]{1,0:T(8,128)}) %all-reduce.16.cloned.1.call-update) | async-done | bytes 262160 | tf_op jit(solution)/shard_map/psum | solution.py:106
  162.8 5.3 %fusion = f32[16,1024]{1,0:T(8,128)} fusion(bf16[4096,1024]{1,0:T(8,128)(2,1)} %param.39, f32[16,4096]{1,0:T(8,128)} %all-reduce.16.cloned.1.call-done, f32[16]{0:T(128)S(1)} %add_rsqrt_fusion), kind=kOutput, calls=%fused_computation.2 | convolution fusion | flops 134479872 | bytes 8716352 | tf_op jit(solution)/shard_map/dot_general | solution.py:25
  168.2 31.6 %all-reduce.18.cloned.1.call-done = f32[16,1024]{1,0:T(8,128)} async-done(((f32[16,1024]{1,0:T(8,128)}), f32[16,1024]{1,0:T(8,128)}) %all-reduce.18.cloned.1.call-update) | async-done | bytes 65552 | tf_op jit(solution)/shard_map/psum | solution.py:110
  199.7 1.5 fusion.8
  (63 shorter events, 0.8 us)
Async XLA Ops:
  7.2 1.6 copy-start
  7.2 3.5 %copy-start.3 = (bf16[16,1024]{1,0:T(8,128)(2,1)S(1)}, bf16[16,1024]{1,0:T(8,128)(2,1)}, u32[]{:S(2)}) copy-start(bf16[16,1024]{1,0:T(8,128)(2,1)} %param.20) | copy-start | bytes 98308
  7.2 42.3 %all-reduce.20.cloned.1.call-start = ((), (), s32[]{:S(2)}) async-start(), calls=%async_computation.3 | async-start | bytes 262144
  7.2 3.4 %copy-start.2 = (bf16[1024,1024]{1,0:T(8,128)(2,1)S(1)}, bf16[1024,1024]{1,0:T(8,128)(2,1)}, u32[]{:S(2)}) copy-start(bf16[1024,1024]{1,0:T(8,128)(2,1)} %param.26) | copy-start | bytes 6291460
  8.8 3.2 %copy-start.15 = (s32[4]{0:T(128)S(1)}, s32[4]{0:T(128)}, u32[]{:S(2)}) copy-start(s32[4]{0:T(128)} %param.21) | copy-start | bytes 52
  8.8 3.2 %copy-start.16 = (f32[16]{0:T(128)S(1)}, f32[16]{0:T(128)}, u32[]{:S(2)}) copy-start(f32[16]{0:T(128)} %param.32) | copy-start | bytes 196
  8.8 3.2 %copy-start.6 = (bf16[1024,16]{0,1:T(8,128)(2,1)S(1)}, bf16[1024,16]{0,1:T(8,128)(2,1)}, u32[]{:S(2)}) copy-start(bf16[1024,16]{0,1:T(8,128)(2,1)} %param.30) | copy-start | bytes 98308
  8.8 3.4 %copy-start.10 = (bf16[4,2,256]{2,1,0:T(2,128)(2,1)S(1)}, bf16[4,2,256]{2,1,0:T(2,128)(2,1)}, u32[]{:S(2)}) copy-start(bf16[4,2,256]{2,1,0:T(2,128)(2,1)} %param.34) | copy-start | bytes 12292
  8.8 3.4 %copy-start.4 = (bf16[1024,256]{1,0:T(8,128)(2,1)S(1)}, bf16[1024,256]{1,0:T(8,128)(2,1)}, u32[]{:S(2)}) copy-start(bf16[1024,256]{1,0:T(8,128)(2,1)} %param.28) | copy-start | bytes 1572868
  8.8 3.5 %copy-start.5 = (bf16[1024,256]{1,0:T(8,128)(2,1)S(1)}, bf16[1024,256]{1,0:T(8,128)(2,1)}, u32[]{:S(2)}) copy-start(bf16[1024,256]{1,0:T(8,128)(2,1)} %param.29) | copy-start | bytes 1572868
  10.7 1.8 copy-start.7
  10.7 1.9 copy-start.13
  10.7 24.6 %copy-start.9 = (bf16[4,3,2,256]{3,2,1,0:T(2,128)(2,1)S(1)}, bf16[4,3,2,256]{3,2,1,0:T(2,128)(2,1)}, u32[]{:S(2)}) copy-start(bf16[4,3,2,256]{3,2,1,0:T(2,128)(2,1)} %param.23) | copy-start | bytes 36868
  10.7 24.8 %copy-start.8 = (bf16[4,3,1024]{2,0,1:T(4,128)(2,1)S(1)}, bf16[4,3,1024]{2,0,1:T(4,128)(2,1)}, u32[]{:S(2)}) copy-start(bf16[4,3,1024]{2,0,1:T(4,128)(2,1)} %param.22) | copy-start | bytes 73732
  10.7 25.6 %copy-start.14 = (f32[16]{0:T(128)S(1)}, f32[16]{0:T(128)}, u32[]{:S(2)}) copy-start(f32[16]{0:T(128)} %param.31) | copy-start | bytes 196
  11.8 108.9 %all-reduce.14.cloned.1.call-start = ((), (), s32[]{:S(2)}) async-start(), calls=%async_computation | async-start | bytes 131072 | tf_op jit(solution)/shard_map/psum | solution.py:99
  52.6 1.3 copy-start.1
  52.6 6.0 %copy-start.11 = (bf16[1024]{0:T(1024)(128)(2,1)S(1)}, bf16[1024]{0:T(1024)(128)(2,1)}, u32[]{:S(2)}) copy-start(bf16[1024]{0:T(1024)(128)(2,1)} %param.35) | copy-start | bytes 6148
  52.6 16.6 %copy-start.12 = (bf16[1024]{0:T(1024)(128)(2,1)S(1)}, bf16[1024]{0:T(1024)(128)(2,1)}, u32[]{:S(2)}) copy-start(bf16[1024]{0:T(1024)(128)(2,1)} %param.37) | copy-start | bytes 6148
  90.7 72.2 %all-reduce.16.cloned.1.call-start = ((), (), s32[]{:S(2)}) async-start(), calls=%async_computation.1 | async-start | bytes 524288 | tf_op jit(solution)/shard_map/psum | solution.py:106
  127.0 72.7 %all-reduce.18.cloned.1.call-start = ((), (), s32[]{:S(2)}) async-start(), calls=%async_computation.2 | async-start | bytes 131072 | tf_op jit(solution)/shard_map/psum | solution.py:110
Sparse Core Ops, SparseCore 0:
  11.9 37.6 all-reduce.19
  90.8 29.8 all-reduce.13
  127.2 35.5 all-reduce.15
  168.3 31.3 all-reduce.17
where the time goes:
time: 208 us
  waiting for transfers between devices  98.7 us (47%)
  blocking collectives  62.5 us (30%)
  matrix products  19.9 us (10%)
  between operations  15.4 us (7%)
  other arithmetic  7.87 us (4%)
  local copies, waits for them, and re-layouts  3.2 us (2%)
    unnamed x2, blocking collectives  31.9 us
    psum x1, waiting for transfers between devices, per_device(): down_sum = lax.psum(product(activation, w_down), 'tp')  31.6 us
    psum x1, waiting for transfers between devices, per_device(): lax.psum((product(all_low, w_out), all_squares), 'tp')  30 us
    psum x1, waiting for transfers between devices, per_device(): lax.psum((product(hidden_low, w_up), row_squares), 'kv')  23.9 us
    dot_general x8, matrix products, product(): return jnp.dot(left, right, preferred_element_type=jnp.float32)  16.6 us
    unnamed x5, waiting for transfers between devices  13.2 us
    all_gather x1, blocking collectives, per_device(): lax.all_gather(gated_low, 'kv', axis=0, tiled=True)  13.1 us
    psum x1, blocking collectives, per_device(): lax.psum((product(hidden_low, w_up), row_squares), 'kv')  11.8 us
  transfers between devices with their start and end apart: 4, of which 4 were waited for; matrix products, arithmetic and copies ran while one was open for 1% of the time, Pallas kernels for 0%

commit v1 on v0

v1 whole, which is shorter than its diff:
```python
import functools

import jax
import jax.numpy as jnp
from jax import lax
from jax.experimental import pallas as pl
from jax.experimental.pallas import tpu as pltpu
from jax.sharding import PartitionSpec as P

D = 4096
HEAD_DIM = 64
STATE = 128
CONV_WIDTH = 4
INNER = 4096
LANES = 128
UP_CHUNKS = 4
TILE = 512

epsilon = 1e-06
F32 = jnp.float32
BF16 = jnp.bfloat16
MESH = pl.DeviceIdType.MESH


def product(left, right):
    return jnp.dot(left, right, preferred_element_type=F32)


def silu(x):
    return x * jax.nn.sigmoid(x)


def tiles(width):
    step = min(TILE, width)
    return [(start, step) for start in range(0, width, step)]


def lane_sum(x):
    return jnp.broadcast_to(jnp.sum(x, axis=1, keepdims=True), (x.shape[0], LANES))


def kernel(
    kv_count,
    tp_count,
    tokens,
    norm_gain,
    mlp_gain,
    inner_gain,
    conv_old,
    conv_tap,
    step_consts,
    ssm_state,
    w_gate,
    w_value,
    w_key,
    w_query,
    w_step,
    w_out,
    w_up,
    w_down,
    layer_out,
    next_state,
    v_gate,
    v_value,
    v_key,
    v_query,
    v_step,
    v_out,
    v_up,
    v_down,
    v_state,
    v_next,
    state_high,
    state_low,
    mix_send,
    mix_recv,
    gate_send,
    gate_recv,
    step_send,
    step_recv,
    low_all,
    low_squares,
    out_all,
    out_squares,
    up_send,
    up_recv,
    up_sq_send,
    up_sq_recv,
    act_all,
    down_all,
    load_sems,
    store_sem,
    kv_send_sems,
    kv_recv_sems,
    tp_send_sems,
    tp_recv_sems,
):
    z = lax.axis_index("kv")
    t = lax.axis_index("tp")
    rows = tokens.shape[0]
    seqs = rows // kv_count
    inner = v_value.shape[1]
    narrow = v_key.shape[1]
    heads = v_step.shape[1]
    group_count = narrow // STATE
    per_group = heads // group_count
    group_width = per_group * HEAD_DIM
    hidden = v_up.shape[1]
    chunk = hidden // UP_CHUNKS

    loads = {}

    def load(name, src, dst):
        copy = pltpu.make_async_copy(src, dst, load_sems.at[len(loads)])
        copy.start()
        loads[name] = copy

    load("value", w_value, v_value)
    load("key", w_key, v_key)
    load("query", w_query, v_query)
    load("step", w_step, v_step)
    load("gate", w_gate, v_gate)
    load("state", ssm_state, v_state)
    load("out", w_out, v_out)

    barrier = pltpu.get_barrier_semaphore()
    for d in range(1, kv_count):
        pl.semaphore_signal(
            barrier, inc=1, device_id={"kv": lax.rem(z + d, kv_count)}, device_id_type=MESH
        )
    for d in range(1, tp_count):
        pl.semaphore_signal(
            barrier, inc=1, device_id={"tp": lax.rem(t + d, tp_count)}, device_id_type=MESH
        )

    started = []

    def exchange(axis, stage, source, target):
        me, count, send_sems, recv_sems = (
            (z, kv_count, kv_send_sems, kv_recv_sems)
            if axis == "kv"
            else (t, tp_count, tp_send_sems, tp_recv_sems)
        )
        copies = []
        for d in range(1, count):
            peer = lax.rem(me + d, count)
            copy = pltpu.make_async_remote_copy(
                src_ref=source(peer),
                dst_ref=target(me),
                send_sem=send_sems.at[stage, d - 1],
                recv_sem=recv_sems.at[stage, d - 1],
                device_id={axis: peer},
                device_id_type=MESH,
            )
            copy.start()
            copies.append(copy)
        started.extend(copies)
        return copies

    def arrive(copies):
        for copy in copies:
            copy.wait_recv()

    def scatter_rows(ref, value, lead=()):
        for j in range(kv_count):
            ref[lead + (j,)] = value[j * seqs : (j + 1) * seqs].astype(ref.dtype)

    def total(ref, count, lead=()):
        acc = ref[lead + (0,)].astype(F32)
        for j in range(1, count):
            acc = acc + ref[lead + (j,)].astype(F32)
        return acc

    def gather_rows(ref, lead=()):
        return jnp.concatenate(
            [ref[lead + (j,)].astype(F32) for j in range(kv_count)], axis=0
        )

    widened = tokens[...].astype(F32)
    scaled = (widened * norm_gain[...].astype(F32)).astype(BF16)
    token_squares = lane_sum(widened * widened)

    def project(weights, send, offset):
        for start, size in tiles(weights.shape[1]):
            piece = product(scaled, weights[:, start : start + size])
            for j in range(kv_count):
                send[j, :, offset + start : offset + start + size] = piece[
                    j * seqs : (j + 1) * seqs
                ].astype(BF16)

    loads["value"].wait()
    project(v_value, mix_send, 0)
    loads["key"].wait()
    project(v_key, mix_send, inner)
    loads["query"].wait()
    project(v_query, mix_send, inner + narrow)
    loads["step"].wait()
    step_part = product(scaled, v_step[...])
    step_part = jnp.concatenate(
        [step_part, jnp.zeros((rows, LANES - heads), F32), token_squares], axis=1
    )
    scatter_rows(step_send, step_part)
    pl.semaphore_wait(barrier, kv_count + tp_count - 2)
    step_copies = exchange("kv", 0, lambda p: step_send.at[p], lambda m: step_recv.at[m])
    mix_copies = exchange("kv", 1, lambda p: mix_send.at[p], lambda m: mix_recv.at[m])
    loads["gate"].wait()
    for c in range(UP_CHUNKS):
        load(
            f"up{c}",
            w_up.at[:, c * chunk : (c + 1) * chunk],
            v_up.at[:, c * chunk : (c + 1) * chunk],
        )
    for c in range(UP_CHUNKS):
        load(
            f"down{c}",
            w_down.at[c * chunk : (c + 1) * chunk],
            v_down.at[c * chunk : (c + 1) * chunk],
        )
    project(v_gate, gate_send, 0)
    gate_copies = exchange("kv", 2, lambda p: gate_send.at[p], lambda m: gate_recv.at[m])
    step_recv[z] = step_send[z]
    mix_recv[z] = mix_send[z]
    gate_recv[z] = gate_send[z]

    loads["state"].wait()
    for b in range(seqs):
        state = v_state[b]
        high = state.astype(BF16)
        state_high[b] = high
        state_low[b] = (state - high.astype(F32)).astype(BF16)

    arrive(step_copies)
    steps = total(step_recv, kv_count)
    inverse = lax.rsqrt(steps[:, LANES : LANES + 1] / D + epsilon)
    step_size = jax.nn.softplus(steps[:, :LANES] * inverse + step_consts[0:1])
    decay = jnp.exp(-jnp.exp(step_consts[1:2]) * step_size)
    head_of = lax.broadcasted_iota(jnp.int32, (LANES, inner), 1) // HEAD_DIM
    one_hot = jnp.where(
        head_of == lax.broadcasted_iota(jnp.int32, (LANES, inner), 0), 1.0, 0.0
    ).astype(F32)
    spread = jnp.dot(
        jnp.concatenate([step_size, decay], axis=0),
        one_hot,
        precision=lax.Precision.HIGHEST,
        preferred_element_type=F32,
    )
    step_wide, decay_wide = spread[:seqs], spread[seqs:]
    arrive(mix_copies)
    mixed = silu(conv_old[...] + total(mix_recv, kv_count) * inverse * conv_tap[...])
    input_wide = step_wide * mixed[:, :inner]
    keys = mixed[:, inner : inner + narrow]
    queries = mixed[:, inner + narrow :]

    pieces = []
    for g in range(group_count):
        query = queries[:, g * STATE : (g + 1) * STATE]
        key = keys[:, g * STATE : (g + 1) * STATE]
        query_high = query.astype(BF16).astype(F32)
        both = jnp.concatenate([query_high, query - query_high], axis=0).astype(BF16)
        lines = []
        for b in range(seqs):
            span = slice(g * per_group, (g + 1) * per_group)
            high = state_high[b, span].reshape(group_width, STATE)
            low = state_low[b, span].reshape(group_width, STATE)
            dims = (((1,), (1,)), ((), ()))
            with_high = lax.dot_general(both, high, dims, preferred_element_type=F32)
            with_low = lax.dot_general(both, low, dims, preferred_element_type=F32)
            lines.append(
                with_high[b : b + 1] + with_high[seqs + b : seqs + b + 1] + with_low[b : b + 1]
            )
        from_state = jnp.concatenate(lines, axis=0)
        overlap = jnp.sum(key * query, axis=1, keepdims=True)
        columns = slice(g * group_width, (g + 1) * group_width)
        pieces.append(decay_wide[:, columns] * from_state + input_wide[:, columns] * overlap)
    mixer_y = jnp.concatenate(pieces, axis=1)
    arrive(gate_copies)
    gated = mixer_y * silu(total(gate_recv, kv_count) * inverse)
    low_all[z] = (gated * inner_gain[...].astype(F32)).astype(BF16)
    low_squares[z] = lane_sum(gated * gated)
    low_copies = exchange("kv", 3, lambda p: low_all.at[z], lambda m: low_all.at[m])
    sq_copies = exchange("kv", 4, lambda p: low_squares.at[z], lambda m: low_squares.at[m])

    padded = jnp.concatenate(
        [input_wide, jnp.zeros((LANES - seqs, inner), F32)], axis=0
    )
    upright = jnp.transpose(padded)
    for b in range(seqs):
        for h in range(heads):
            g = h // per_group
            v_next[b, h] = (
                v_state[b, h] * decay[b : b + 1, h : h + 1]
                + upright[h * HEAD_DIM : (h + 1) * HEAD_DIM, b : b + 1]
                * keys[b : b + 1, g * STATE : (g + 1) * STATE]
            )
    store = pltpu.make_async_copy(v_next, next_state, store_sem)
    store.start()

    loads["out"].wait()
    arrive(low_copies)
    lows = gather_rows(low_all).astype(BF16)
    for start, size in tiles(v_out.shape[1]):
        out_all[t, :, start : start + size] = product(
            lows, v_out[:, start : start + size]
        ).astype(BF16)
    arrive(sq_copies)
    out_squares[t] = gather_rows(low_squares)
    out_copies = exchange("tp", 0, lambda p: out_all.at[t], lambda m: out_all.at[m])
    out_sq_copies = exchange("tp", 1, lambda p: out_squares.at[t], lambda m: out_squares.at[m])
    arrive(out_sq_copies)
    out_inverse = lax.rsqrt(total(out_squares, tp_count)[:, :1] / INNER + epsilon)
    arrive(out_copies)
    residual = (widened + total(out_all, tp_count) * out_inverse).astype(BF16).astype(F32)
    hidden_low = (residual * mlp_gain[...].astype(F32)).astype(BF16)
    scatter_rows(up_sq_send, lane_sum(residual * residual))
    up_sq_copies = exchange("kv", 5, lambda p: up_sq_send.at[p], lambda m: up_sq_recv.at[m])

    up_copies = []
    for c in range(UP_CHUNKS):
        loads[f"up{c}"].wait()
        for start, size in tiles(chunk):
            base = c * chunk + start
            piece = product(hidden_low, v_up[:, base : base + size])
            for j in range(kv_count):
                up_send[c, j, :, start : start + size] = piece[
                    j * seqs : (j + 1) * seqs
                ].astype(BF16)
        up_copies.append(
            exchange(
                "kv",
                6 + c,
                lambda p, c=c: up_send.at[c, p],
                lambda m, c=c: up_recv.at[c, m],
            )
        )
        up_recv[c, z] = up_send[c, z]
    up_sq_recv[z] = up_sq_send[z]
    arrive(up_sq_copies)
    up_inverse = lax.rsqrt(total(up_sq_recv, kv_count)[:, :1] / D + epsilon)
    act_copies = []
    for c in range(UP_CHUNKS):
        arrive(up_copies[c])
        active = jnp.maximum(total(up_recv, kv_count, (c,)) * up_inverse, 0.0)
        act_all[c, z] = (active * active).astype(BF16)
        act_copies.append(
            exchange(
                "kv",
                6 + UP_CHUNKS + c,
                lambda p, c=c: act_all.at[c, z],
                lambda m, c=c: act_all.at[c, m],
            )
        )
    down = jnp.zeros((rows, v_down.shape[1]), F32)
    for c in range(UP_CHUNKS):
        loads[f"down{c}"].wait()
        arrive(act_copies[c])
        acts = gather_rows(act_all, (c,)).astype(BF16)
        down = down + product(acts, v_down[c * chunk : (c + 1) * chunk])
    down_all[t] = down.astype(BF16)
    down_copies = exchange("tp", 2, lambda p: down_all.at[t], lambda m: down_all.at[m])
    arrive(down_copies)
    layer_out[...] = (residual + total(down_all, tp_count)).astype(BF16)
    for copy in started:
        copy.wait_send()
    store.wait()


def per_device(
    kv_count,
    tp_count,
    tokens,
    lengths,
    conv_state_x,
    conv_state_bc,
    ssm_state,
    norm_gain,
    w_gate,
    w_value,
    w_key,
    w_query,
    w_step,
    step_bias,
    decay_log,
    conv_x,
    conv_bc,
    inner_gain,
    w_out,
    mlp_gain,
    w_up,
    w_down,
):
    rows, depth = tokens.shape
    seqs = lengths.shape[0]
    inner, narrow, heads = w_value.shape[1], w_key.shape[1], w_step.shape[1]
    hidden = w_up.shape[1]
    chunk = hidden // UP_CHUNKS
    row_live = (
        jnp.arange(CONV_WIDTH - 1, dtype=jnp.int32)[None, :] >= CONV_WIDTH - 1 - lengths[:, None]
    ).astype(F32)
    taps = jnp.concatenate([conv_x, conv_bc.reshape(CONV_WIDTH, 2 * narrow)], axis=1).astype(F32)
    held = jnp.concatenate(
        [conv_state_x, conv_state_bc.reshape(seqs, CONV_WIDTH - 1, 2 * narrow)], axis=2
    ).astype(F32)
    conv_old = jnp.zeros((seqs, inner + 2 * narrow), F32)
    for k in range(CONV_WIDTH - 1):
        conv_old = conv_old + held[:, k] * row_live[:, k][:, None] * taps[k]
    conv_tap = taps[CONV_WIDTH - 1 :]
    step_consts = jnp.pad(jnp.stack([step_bias, decay_log]), ((0, 0), (0, LANES - heads)))

    vmem = pl.BlockSpec(memory_space=pltpu.VMEM)
    hbm = pl.BlockSpec(memory_space=pl.ANY)
    mixed = inner + 2 * narrow
    width = w_out.shape[1]
    stages = 6 + 2 * UP_CHUNKS
    return pl.pallas_call(
        functools.partial(kernel, kv_count, tp_count),
        out_shape=(
            jax.ShapeDtypeStruct((rows, width), BF16),
            jax.ShapeDtypeStruct(ssm_state.shape, F32),
        ),
        in_specs=[vmem] * 7 + [hbm] * 9,
        out_specs=(vmem, hbm),
        scratch_shapes=[
            pltpu.VMEM(w_gate.shape, BF16),
            pltpu.VMEM(w_value.shape, BF16),
            pltpu.VMEM(w_key.shape, BF16),
            pltpu.VMEM(w_query.shape, BF16),
            pltpu.VMEM(w_step.shape, BF16),
            pltpu.VMEM(w_out.shape, BF16),
            pltpu.VMEM(w_up.shape, BF16),
            pltpu.VMEM(w_down.shape, BF16),
            pltpu.VMEM(ssm_state.shape, F32),
            pltpu.VMEM(ssm_state.shape, F32),
            pltpu.VMEM(ssm_state.shape, BF16),
            pltpu.VMEM(ssm_state.shape, BF16),
            pltpu.VMEM((kv_count, seqs, mixed), BF16),
            pltpu.VMEM((kv_count, seqs, mixed), BF16),
            pltpu.VMEM((kv_count, seqs, inner), BF16),
            pltpu.VMEM((kv_count, seqs, inner), BF16),
            pltpu.VMEM((kv_count, seqs, 2 * LANES), F32),
            pltpu.VMEM((kv_count, seqs, 2 * LANES), F32),
            pltpu.VMEM((kv_count, seqs, inner), BF16),
            pltpu.VMEM((kv_count, seqs, LANES), F32),
            pltpu.VMEM((tp_count, rows, width), BF16),
            pltpu.VMEM((tp_count, rows, LANES), F32),
            pltpu.VMEM((UP_CHUNKS, kv_count, seqs, chunk), BF16),
            pltpu.VMEM((UP_CHUNKS, kv_count, seqs, chunk), BF16),
            pltpu.VMEM((kv_count, seqs, LANES), F32),
            pltpu.VMEM((kv_count, seqs, LANES), F32),
            pltpu.VMEM((UP_CHUNKS, kv_count, seqs, chunk), BF16),
            pltpu.VMEM((tp_count, rows, width), BF16),
            pltpu.SemaphoreType.DMA((7 + 2 * UP_CHUNKS,)),
            pltpu.SemaphoreType.DMA,
            pltpu.SemaphoreType.DMA((stages, max(kv_count - 1, 1))),
            pltpu.SemaphoreType.DMA((stages, max(kv_count - 1, 1))),
            pltpu.SemaphoreType.DMA((3, max(tp_count - 1, 1))),
            pltpu.SemaphoreType.DMA((3, max(tp_count - 1, 1))),
        ],
        compiler_params=pltpu.CompilerParams(
            collective_id=0, has_side_effects=True, vmem_limit_bytes=60 * 1024 * 1024
        ),
    )(
        tokens,
        norm_gain[None],
        mlp_gain[None],
        inner_gain[None],
        conv_old,
        conv_tap,
        step_consts,
        ssm_state,
        w_gate,
        w_value,
        w_key,
        w_query,
        w_step,
        w_out,
        w_up,
        w_down,
    )


def solution(mesh):
    return jax.shard_map(
        functools.partial(per_device, mesh.shape["kv"], mesh.shape["tp"]),
        mesh=mesh,
        in_specs=(
            P("grp", "kv"),
            P(("grp", "kv")),
            P(("grp", "kv"), None, "tp"),
            P(("grp", "kv"), None, None, "tp"),
            P(("grp", "kv"), "tp", None, None),
            P("kv"),
            P("kv", "tp"),
            P("kv", "tp"),
            P("kv", "tp"),
            P("kv", "tp"),
            P("kv", "tp"),
            P("tp"),
            P("tp"),
            P(None, "tp"),
            P(None, None, "tp"),
            P("tp"),
            P("tp", "kv"),
            P("kv"),
            P("kv", "tp"),
            P("tp", "kv"),
        ),
        out_specs=(P("grp", "kv"), P(("grp", "kv"), "tp", None, None)),
        check_vma=False,
    )
```

time: 208 us -> 50 us (0.24)
  waiting for transfers between devices: 98.7 us -> 0 us
  blocking collectives: 62.5 us -> 0 us
  Pallas kernels: 0 us -> 32.6 us
  matrix products: 19.9 us -> 0 us
  between operations: 15.4 us -> 0.66 us
  local copies, waits for them, and re-layouts: 3.2 us -> 12 us
  other arithmetic: 7.87 us -> 4.08 us
    psum x3 -> x0, waiting for transfers between devices: 85.5 us -> none  [the longest x1 31.6 us: per_device(): down_sum = lax.psum(product(activation, w_down), 'tp')]
    pallas_call x0 -> x1, Pallas kernels: none -> 32.6 us  [per_device(): pl.pallas_call(functools.partial(kernel, kv_count, tp_count), out_shape=(...]
    unnamed x2 -> x0, blocking collectives: 31.9 us -> none
    dot_general x9 -> x0, matrix products: 19.9 us -> none  [the longest x8 16.6 us: product(): return jnp.dot(left, right, preferred_element_type=jnp.float32)]
    psum x2 -> x0, blocking collectives: 17.5 us -> none  [the longest x1 11.8 us: per_device(): lax.psum((product(hidden_low, w_up), row_squares), 'kv')]
    unnamed x5 -> x0, waiting for transfers between devices: 13.2 us -> none
    all_gather x1 -> x0, blocking collectives: 13.1 us -> none  [per_device(): lax.all_gather(gated_low, 'kv', axis=0, tiled=True)]
    unnamed x38 -> x5, local copies, waits for them, and re-layouts: 2.98 us -> 7.54 us
  transfers between devices with their start and end apart: 4 -> 0, of which waited for: 4 -> 0; matrix products, arithmetic and copies ran while one was open for 1% -> 0% of each run, Pallas kernels for 0% -> 0%
where the time goes in v1:
time: 50 us; the launch traced here: 49.4 us
  Pallas kernels  32.6 us (65%)
  local copies, waits for them, and re-layouts  12 us (24%)
  other arithmetic  4.08 us (8%)
  between operations  0.66 us (1%)
    pallas_call x1, Pallas kernels, per_device(): pl.pallas_call(functools.partial(kernel, kv_count, tp_count), out_shape=(...  32.6 us
    unnamed x5, local copies, waits for them, and re-layouts  7.54 us
    broadcast_in_dim x1, local copies, waits for them, and re-layouts, per_device(): mlp_gain[None]  1.28 us
    broadcast_in_dim x1, local copies, waits for them, and re-layouts, per_device(): norm_gain[None]  1.28 us
    broadcast_in_dim x1, local copies, waits for them, and re-layouts, per_device(): inner_gain[None]  1.27 us
    another operation x1, other arithmetic, per_device(): jnp.stack([step_bias, decay_log])  1.27 us

profile of v1, /device:TPU:0, one launch (start us, length us, event | category | flops | bytes accessed | tf_op | source)
XLA Modules:
  0.0 49.4 jit_solution(15732268862709571527)
XLA Ops:
  0.6 0.7 %broadcast_subtract_fusion = s32[4]{0:T(128)S(1)} fusion(s32[4]{0:T(128)} %param.21), kind=kLoop, calls=%fused_computation.22 | loop fusion | flops 4 | bytes 32 | tf_op jit(solution)/shard_map/sub | solution.py:397
  1.3 1.3 %select_maximum_fusion.step_consts = f32[2,128]{1,0:T(2,128)} fusion(f32[1,16]{1,0:T(1,128)} %bitcast.40, f32[1,16]{1,0:T(1,128)} %bitcast.41), kind=kLoop, calls=%fused_computation.18 | loop fusion | flops 1024 | bytes 1152 | tf_op jit(solution)/shard_map/stack | solution.py:407
  2.6 1.3 %broadcast_in_dim.11.norm_gain = bf16[1,1024]{1,0:T(2,128)(2,1)} reshape(bf16[1024]{0:T(1024)(128)(2,1)} %param.25) | data formatting | bytes 4096 | tf_op jit(solution)/shard_map/broadcast_in_dim | solution.py:463
  3.8 0.7 %copy.24 = bf16[1,4,2,256]{3,1,2,0:T(4,128)(2,1)S(1)} copy(bf16[1,4,2,256]{3,2,1,0:T(2,128)(2,1)} %bitcast.39) | data formatting | bytes 8192
  4.5 1.3 %broadcast_in_dim.13.inner_gain = bf16[1,1024]{1,0:T(2,128)(2,1)} reshape(bf16[1024]{0:T(1024)(128)(2,1)} %param.35) | data formatting | bytes 4096 | tf_op jit(solution)/shard_map/broadcast_in_dim | solution.py:465
  5.8 1.3 %broadcast_in_dim.12.mlp_gain = bf16[1,1024]{1,0:T(2,128)(2,1)} reshape(bf16[1024]{0:T(1024)(128)(2,1)} %param.37) | data formatting | bytes 4096 | tf_op jit(solution)/shard_map/broadcast_in_dim | solution.py:464
  7.1 0.7 %copy.22 = bf16[4,3,2,256]{3,2,0,1:T(2,128)(2,1)S(1)} copy(bf16[4,3,2,256]{3,2,1,0:T(2,128)(2,1)} %param.23) | data formatting | bytes 24576 | tf_op args[3]
  7.8 0.7 %maximum_convert_fusion.1 = f32[4,1536]{1,0:T(4,128)S(1)} fusion(bf16[4,512]{1,0:T(4,128)(2,1)S(1)} %bitcast.38, bf16[4,1024]{1,0:T(4,128)(2,1)} %param.33), kind=kLoop, calls=%fused_computation.12 | loop fusion | flops 24576 | bytes 36864 | tf_op jit(solution)/shard_map/convert_element_type | solution.py:399
  8.5 0.6 %slice_reduce_fusion.2 = (f32[1536]{0:T(1024)S(1)}, f32[1536]{0:T(1024)S(1)}, f32[1536]{0:T(1024)S(1)}, f32[1,1536]{1,0:T(1,128)}) fusion(f32[4,1536]{1,0:T(4,128)S(1)} %maximum_convert_fusion.1), kind=kLoop, calls=%fused_computation.15 | loop fusion | bytes 49152 | tf_op jit(solution)/shard_map/slice | solution.py:405
  9.1 0.8 %maximum_convert_fusion = f32[4,3,1536]{2,0,1:T(4,128)S(1)} fusion(bf16[4,3,512]{2,0,1:T(4,128)(2,1)S(1)} %reshape.12, bf16[4,3,1024]{2,0,1:T(4,128)(2,1)} %param.22), kind=kLoop, calls=%fused_computation | loop fusion | flops 73728 | bytes 110592 | tf_op jit(solution)/shard_map/convert_element_type | solution.py:402
  9.9 0.7 %fusion.2.conv_old = f32[4,1536]{1,0:T(4,128)} fusion(f32[4,3,1536]{2,0,1:T(4,128)S(1)} %maximum_convert_fusion, f32[1536]{0:T(1024)S(1)} %get-tuple-element.3, f32[4]{0:T(128)S(1)} %get-tuple-element.7, f32[1536]{0:T(1024)S(1)} %get-tuple-element.4, f32[4]{0:T(128)S(1)} %get-tuple-element.8, f32[1536]{0:T(1024)S(1)} %get-tuple-element.2, ...), kind=kLoop, calls=%fused_computation.4 | loop fusion | flops 49152 | bytes 116784 | tf_op jit(solution)/shard_map/add | solution.py:405
  10.6 1.6 %copy.23.w_step = bf16[1024,16]{1,0:T(8,128)(2,1)} copy(bf16[1024,16]{0,1:T(8,128)(2,1)} %param.30) | data formatting | bytes 65536 | tf_op args[10]
  12.2 32.6 %shard_map.203 = (bf16[16,1024]{1,0:T(8,128)(2,1)}, f32[4,16,64,128]{3,2,1,0:T(8,128)}) custom-call(bf16[16,1024]{1,0:T(8,128)(2,1)} %tokens.1, bf16[1,1024]{1,0:T(2,128)(2,1)} %broadcast_in_dim.11.norm_gain, bf16[1,1024]{1,0:T(2,128)(2,1)} %broadcast_in_dim.12.mlp_gain, bf16[1,1024]{1,0:T(2,128)(2,1)} %broadcast_in_dim.13.inner_gain, ...), custom_call_target="tpu_custom_call" | custom-call | tf_op jit(solution)/shard_map/pallas_call | solution.py:414
  44.8 1.4 %copy.27 = bf16[16,1024]{1,0:T(8,128)(2,1)} copy(bf16[16,1024]{1,0:T(8,128)(2,1)} %get-tuple-element.11) | data formatting | bytes 65536
  46.2 3.2 %copy.28 = f32[4,16,64,128]{3,2,1,0:T(8,128)} copy(f32[4,16,64,128]{3,2,1,0:T(8,128)} %get-tuple-element.12) | data formatting | bytes 4194304
  (3 shorter events, 0.0 us)

commit v2 on v1

--- a/solution.py
+++ b/solution.py
@@ -13,6 +13,7 @@
 CONV_WIDTH = 4
 INNER = 4096
 LANES = 128
+VMEM_BYTES = 67043328
 UP_CHUNKS = 4
 TILE = 512
 
@@ -42,13 +43,17 @@
 def kernel(
     kv_count,
     tp_count,
-    tokens,
-    norm_gain,
-    mlp_gain,
-    inner_gain,
-    conv_old,
-    conv_tap,
-    step_consts,
+    h_tokens,
+    h_lengths,
+    h_conv_state_x,
+    h_conv_state_bc,
+    h_norm_gain,
+    h_mlp_gain,
+    h_inner_gain,
+    h_step_bias,
+    h_decay_log,
+    h_conv_x,
+    h_conv_bc,
     ssm_state,
     w_gate,
     w_value,
@@ -69,9 +74,19 @@
     v_up,
     v_down,
     v_state,
-    v_next,
     state_high,
     state_low,
+    tokens,
+    lengths,
+    conv_state_x,
+    conv_state_bc,
+    norm_gain,
+    mlp_gain,
+    inner_gain,
+    step_bias,
+    decay_log,
+    conv_x,
+    conv_bc,
     mix_send,
     mix_recv,
     gate_send,
@@ -89,7 +104,6 @@
     act_all,
     down_all,
     load_sems,
-    store_sem,
     kv_send_sems,
     kv_recv_sems,
     tp_send_sems,
@@ -101,7 +115,7 @@
     seqs = rows // kv_count
     inner = v_value.shape[1]
     narrow = v_key.shape[1]
-    heads = v_step.shape[1]
+    heads = v_step.shape[0]
     group_count = narrow // STATE
     per_group = heads // group_count
     group_width = per_group * HEAD_DIM
@@ -115,11 +129,26 @@
         copy.start()
         loads[name] = copy
 
+    load("tokens", h_tokens, tokens)
+    load("norm_gain", h_norm_gain, norm_gain)
     load("value", w_value, v_value)
     load("key", w_key, v_key)
     load("query", w_query, v_query)
     load("step", w_step, v_step)
     load("gate", w_gate, v_gate)
+    small = [
+        ("lengths", h_lengths, lengths),
+        ("conv_state_x", h_conv_state_x, conv_state_x),
+        ("conv_state_bc", h_conv_state_bc, conv_state_bc),
+        ("mlp_gain", h_mlp_gain, mlp_gain),
+        ("inner_gain", h_inner_gain, inner_gain),
+        ("step_bias", h_step_bias, step_bias),
+        ("decay_log", h_decay_log, decay_log),
+        ("conv_x", h_conv_x, conv_x),
+        ("conv_bc", h_conv_bc, conv_bc),
+    ]
+    for item in small:
+        load(*item)
     load("state", ssm_state, v_state)
     load("out", w_out, v_out)
 
@@ -176,8 +205,13 @@
             [ref[lead + (j,)].astype(F32) for j in range(kv_count)], axis=0
         )
 
+    def gain(ref):
+        return ref[...].astype(F32).reshape(1, ref.shape[0])
+
+    loads["tokens"].wait()
+    loads["norm_gain"].wait()
     widened = tokens[...].astype(F32)
-    scaled = (widened * norm_gain[...].astype(F32)).astype(BF16)
+    scaled = (widened * gain(norm_gain)).astype(BF16)
     token_squares = lane_sum(widened * widened)
 
     def project(weights, send, offset):
@@ -195,7 +229,9 @@
     loads["query"].wait()
     project(v_query, mix_send, inner + narrow)
     loads["step"].wait()
-    step_part = product(scaled, v_step[...])
+    step_part = lax.dot_general(
+        scaled, v_step[...], (((1,), (1,)), ((), ())), preferred_element_type=F32
+    )
     step_part = jnp.concatenate(
         [step_part, jnp.zeros((rows, LANES - heads), F32), token_squares], axis=1
     )
@@ -229,11 +265,38 @@
         state_high[b] = high
         state_low[b] = (state - high.astype(F32)).astype(BF16)
 
+    for name, _, _ in small:
+        loads[name].wait()
+    seq_of = lax.broadcasted_iota(jnp.int32, (seqs, 1), 0)
+    seen = jnp.zeros((seqs, 1), jnp.int32)
+    for b in range(seqs):
+        seen = jnp.where(seq_of == b, lengths[b], seen)
+    lane_of = lax.broadcasted_iota(jnp.int32, (1, LANES), 1)
+    bias_row = jnp.zeros((1, LANES), F32)
+    log_row = jnp.zeros((1, LANES), F32)
+    for h in range(heads):
+        bias_row = jnp.where(lane_of == h, step_bias[h], bias_row)
+        log_row = jnp.where(lane_of == h, decay_log[h], log_row)
+
+    taps = jnp.concatenate(
+        [conv_x[...].astype(F32)] + [conv_bc[:, i].astype(F32) for i in range(2)], axis=1
+    )
+    conv_old = jnp.zeros((seqs, inner + 2 * narrow), F32)
+    for k in range(CONV_WIDTH - 1):
+        held = jnp.concatenate(
+            [conv_state_x[k].astype(F32)]
+            + [conv_state_bc[:, k, i].astype(F32) for i in range(2)],
+            axis=1,
+        )
+        live = jnp.where(seen >= CONV_WIDTH - 1 - k, 1.0, 0.0)
+        conv_old = conv_old + held * live * taps[k : k + 1]
+    conv_tap = taps[CONV_WIDTH - 1 :]
+
     arrive(step_copies)
     steps = total(step_recv, kv_count)
     inverse = lax.rsqrt(steps[:, LANES : LANES + 1] / D + epsilon)
-    step_size = jax.nn.softplus(steps[:, :LANES] * inverse + step_consts[0:1])
-    decay = jnp.exp(-jnp.exp(step_consts[1:2]) * step_size)
+    step_size = jax.nn.softplus(steps[:, :LANES] * inverse + bias_row)
+    decay = jnp.exp(-jnp.exp(log_row) * step_size)
     head_of = lax.broadcasted_iota(jnp.int32, (LANES, inner), 1) // HEAD_DIM
     one_hot = jnp.where(
         head_of == lax.broadcasted_iota(jnp.int32, (LANES, inner), 0), 1.0, 0.0
@@ -246,7 +309,7 @@
     )
     step_wide, decay_wide = spread[:seqs], spread[seqs:]
     arrive(mix_copies)
-    mixed = silu(conv_old[...] + total(mix_recv, kv_count) * inverse * conv_tap[...])
+    mixed = silu(conv_old + total(mix_recv, kv_count) * inverse * conv_tap)
     input_wide = step_wide * mixed[:, :inner]
     keys = mixed[:, inner : inner + narrow]
     queries = mixed[:, inner + narrow :]
@@ -275,7 +338,7 @@
     mixer_y = jnp.concatenate(pieces, axis=1)
     arrive(gate_copies)
     gated = mixer_y * silu(total(gate_recv, kv_count) * inverse)
-    low_all[z] = (gated * inner_gain[...].astype(F32)).astype(BF16)
+    low_all[z] = (gated * gain(inner_gain)).astype(BF16)
     low_squares[z] = lane_sum(gated * gated)
     low_copies = exchange("kv", 3, lambda p: low_all.at[z], lambda m: low_all.at[m])
     sq_copies = exchange("kv", 4, lambda p: low_squares.at[z], lambda m: low_squares.at[m])
@@ -287,13 +350,11 @@
     for b in range(seqs):
         for h in range(heads):
             g = h // per_group
-            v_next[b, h] = (
+            next_state[b, h] = (
                 v_state[b, h] * decay[b : b + 1, h : h + 1]
                 + upright[h * HEAD_DIM : (h + 1) * HEAD_DIM, b : b + 1]
                 * keys[b : b + 1, g * STATE : (g + 1) * STATE]
             )
-    store = pltpu.make_async_copy(v_next, next_state, store_sem)
-    store.start()
 
     loads["out"].wait()
     arrive(low_copies)
@@ -310,7 +371,7 @@
     out_inverse = lax.rsqrt(total(out_squares, tp_count)[:, :1] / INNER + epsilon)
     arrive(out_copies)
     residual = (widened + total(out_all, tp_count) * out_inverse).astype(BF16).astype(F32)
-    hidden_low = (residual * mlp_gain[...].astype(F32)).astype(BF16)
+    hidden_low = (residual * gain(mlp_gain)).astype(BF16)
     scatter_rows(up_sq_send, lane_sum(residual * residual))
     up_sq_copies = exchange("kv", 5, lambda p: up_sq_send.at[p], lambda m: up_sq_recv.at[m])
 
@@ -361,7 +422,6 @@
     layer_out[...] = (residual + total(down_all, tp_count)).astype(BF16)
     for copy in started:
         copy.wait_send()
-    store.wait()
 
 
 def per_device(
@@ -393,45 +453,44 @@
     inner, narrow, heads = w_value.shape[1], w_key.shape[1], w_step.shape[1]
     hidden = w_up.shape[1]
     chunk = hidden // UP_CHUNKS
-    row_live = (
-        jnp.arange(CONV_WIDTH - 1, dtype=jnp.int32)[None, :] >= CONV_WIDTH - 1 - lengths[:, None]
-    ).astype(F32)
-    taps = jnp.concatenate([conv_x, conv_bc.reshape(CONV_WIDTH, 2 * narrow)], axis=1).astype(F32)
-    held = jnp.concatenate(
-        [conv_state_x, conv_state_bc.reshape(seqs, CONV_WIDTH - 1, 2 * narrow)], axis=2
-    ).astype(F32)
-    conv_old = jnp.zeros((seqs, inner + 2 * narrow), F32)
-    for k in range(CONV_WIDTH - 1):
-        conv_old = conv_old + held[:, k] * row_live[:, k][:, None] * taps[k]
-    conv_tap = taps[CONV_WIDTH - 1 :]
-    step_consts = jnp.pad(jnp.stack([step_bias, decay_log]), ((0, 0), (0, LANES - heads)))
-
+    results = 4 * ssm_state.size + 2 * rows * w_out.shape[1]
+    grant = (VMEM_BYTES - results) // 4096 * 4096 - 4096
     vmem = pl.BlockSpec(memory_space=pltpu.VMEM)
-    hbm = pl.BlockSpec(memory_space=pl.ANY)
+    hbm = pl.BlockSpec(memory_space=pltpu.HBM)
     mixed = inner + 2 * narrow
     width = w_out.shape[1]
     stages = 6 + 2 * UP_CHUNKS
     return pl.pallas_call(
         functools.partial(kernel, kv_count, tp_count),
         out_shape=(
-            jax.ShapeDtypeStruct((rows, width), BF16),
-            jax.ShapeDtypeStruct(ssm_state.shape, F32),
+            pltpu.VMEM((rows, width), BF16),
+            pltpu.VMEM(ssm_state.shape, F32),
         ),
-        in_specs=[vmem] * 7 + [hbm] * 9,
-        out_specs=(vmem, hbm),
+        in_specs=[hbm] * 20,
+        out_specs=(vmem, vmem),
         scratch_shapes=[
             pltpu.VMEM(w_gate.shape, BF16),
             pltpu.VMEM(w_value.shape, BF16),
             pltpu.VMEM(w_key.shape, BF16),
             pltpu.VMEM(w_query.shape, BF16),
-            pltpu.VMEM(w_step.shape, BF16),
+            pltpu.VMEM(w_step.shape[::-1], BF16),
             pltpu.VMEM(w_out.shape, BF16),
             pltpu.VMEM(w_up.shape, BF16),
             pltpu.VMEM(w_down.shape, BF16),
             pltpu.VMEM(ssm_state.shape, F32),
-            pltpu.VMEM(ssm_state.shape, F32),
             pltpu.VMEM(ssm_state.shape, BF16),
             pltpu.VMEM(ssm_state.shape, BF16),
+            pltpu.VMEM(tokens.shape, BF16),
+            pltpu.SMEM(lengths.shape, jnp.int32),
+            pltpu.VMEM((CONV_WIDTH - 1, seqs, inner), BF16),
+            pltpu.VMEM(conv_state_bc.shape, BF16),
+            pltpu.VMEM(norm_gain.shape, BF16),
+            pltpu.VMEM(mlp_gain.shape, BF16),
+            pltpu.VMEM(inner_gain.shape, BF16),
+            pltpu.SMEM(step_bias.shape, F32),
+            pltpu.SMEM(decay_log.shape, F32),
+            pltpu.VMEM(conv_x.shape, BF16),
+            pltpu.VMEM(conv_bc.shape, BF16),
             pltpu.VMEM((kv_count, seqs, mixed), BF16),
             pltpu.VMEM((kv_count, seqs, mixed), BF16),
             pltpu.VMEM((kv_count, seqs, inner), BF16),
@@ -448,30 +507,33 @@
             pltpu.VMEM((kv_count, seqs, LANES), F32),
             pltpu.VMEM((UP_CHUNKS, kv_count, seqs, chunk), BF16),
             pltpu.VMEM((tp_count, rows, width), BF16),
-            pltpu.SemaphoreType.DMA((7 + 2 * UP_CHUNKS,)),
-            pltpu.SemaphoreType.DMA,
+            pltpu.SemaphoreType.DMA((18 + 2 * UP_CHUNKS,)),
             pltpu.SemaphoreType.DMA((stages, max(kv_count - 1, 1))),
             pltpu.SemaphoreType.DMA((stages, max(kv_count - 1, 1))),
             pltpu.SemaphoreType.DMA((3, max(tp_count - 1, 1))),
             pltpu.SemaphoreType.DMA((3, max(tp_count - 1, 1))),
         ],
         compiler_params=pltpu.CompilerParams(
-            collective_id=0, has_side_effects=True, vmem_limit_bytes=60 * 1024 * 1024
+            collective_id=0, has_side_effects=True, vmem_limit_bytes=grant
         ),
     )(
         tokens,
-        norm_gain[None],
-        mlp_gain[None],
-        inner_gain[None],
-        conv_old,
-        conv_tap,
-        step_consts,
+        lengths,
+        jnp.swapaxes(conv_state_x, 0, 1),
+        conv_state_bc,
+        norm_gain,
+        mlp_gain,
+        inner_gain,
+        step_bias,
+        decay_log,
+        conv_x,
+        conv_bc,
         ssm_state,
         w_gate,
         w_value,
         w_key,
         w_query,
-        w_step,
+        w_step.T,
         w_out,
         w_up,
         w_down,

time: 50 us -> 34 us (0.68); the launches traced: 49.4 us -> 33.9 us
  local copies, waits for them, and re-layouts: 12 us -> 1.94 us
  other arithmetic: 4.08 us -> 0 us
  Pallas kernels: 32.6 us -> 31.3 us
    unnamed x5 -> x2, local copies, waits for them, and re-layouts: 7.54 us -> 1.94 us
    broadcast_in_dim x3 -> x0, local copies, waits for them, and re-layouts: 3.82 us -> none  [the longest x1 1.28 us: per_device(): mlp_gain[None]]
    convert_element_type x3 -> x0, other arithmetic: 1.46 us -> none  [the longest x1 0.75 us: per_device(): held = jnp.concatenate([conv_state_x, conv_state_bc.reshape(seqs, CONV_WI...]
    pallas_call x1, Pallas kernels: 32.6 us -> 31.3 us  [per_device(): pl.pallas_call(functools.partial(kernel, kv_count, tp_count), out_shape=(...]
    another operation x1 -> x0, other arithmetic: 1.27 us -> none  [per_device(): jnp.stack([step_bias, decay_log])]
    add x1 -> x0, other arithmetic: 0.69 us -> none  [per_device(): conv_old = conv_old + held[:, k] * row_live[:, k][:, None] * taps[k]]
    sub x1 -> x0, other arithmetic: 0.66 us -> none  [per_device(): CONV_WIDTH - 1 - lengths[:, None]]
    slice x1 -> x0, local copies, waits for them, and re-layouts: 0.61 us -> none  [per_device(): conv_old = conv_old + held[:, k] * row_live[:, k][:, None] * taps[k]]
where the time goes in v2:
time: 34 us; the launch traced here: 33.9 us
  Pallas kernels  31.3 us (92%)
  local copies, waits for them, and re-layouts  1.94 us (6%)
  between operations  0.65 us (2%)
    pallas_call x1, Pallas kernels, per_device(): pl.pallas_call(functools.partial(kernel, kv_count, tp_count), out_shape=(...  31.3 us
    unnamed x2, local copies, waits for them, and re-layouts  1.94 us

profile of v2, /device:TPU:0, one launch (start us, length us, event | category | flops | bytes accessed | tf_op | source)
XLA Modules:
  0.0 33.9 jit_solution(13536203294243853010)
XLA Ops:
  0.6 31.3 %shard_map.203 = (bf16[16,1024]{1,0:T(8,128)(2,1)S(1)}, f32[4,16,64,128]{3,2,1,0:T(8,128)S(1)}) custom-call(bf16[16,1024]{1,0:T(8,128)(2,1)} %h_tokens.1, s32[4]{0:T(128)} %h_lengths.1, bf16[3,4,1024]{2,1,0:T(4,128)(2,1)} %bitcast.3, bf16[4,3,2,256]{3,2,1,0:T(2,128)(2,1)} %h_conv_state_bc.1, bf16[1024]{0:T(1024)(128)(2,1)} %h_norm_gain.1, ...), custom_call_target="tpu_custom_call" | custom-call | tf_op jit(solution)/shard_map/pallas_call | solution.py:463
  32.0 0.6 %copy.24 = bf16[16,1024]{1,0:T(8,128)(2,1)} copy(bf16[16,1024]{1,0:T(8,128)(2,1)S(1)} %get-tuple-element.2) | data formatting | bytes 65536
  32.6 1.3 %copy.25 = f32[4,16,64,128]{3,2,1,0:T(8,128)} copy(f32[4,16,64,128]{3,2,1,0:T(8,128)S(1)} %get-tuple-element.3) | data formatting | bytes 4194304

commit v3 on v2

--- a/solution.py
+++ b/solution.py
@@ -347,14 +347,17 @@
         [input_wide, jnp.zeros((LANES - seqs, inner), F32)], axis=0
     )
     upright = jnp.transpose(padded)
-    for b in range(seqs):
-        for h in range(heads):
-            g = h // per_group
-            next_state[b, h] = (
-                v_state[b, h] * decay[b : b + 1, h : h + 1]
-                + upright[h * HEAD_DIM : (h + 1) * HEAD_DIM, b : b + 1]
-                * keys[b : b + 1, g * STATE : (g + 1) * STATE]
-            )
+    def update(first, last):
+        for b in range(seqs * first // 4, seqs * last // 4):
+            for h in range(heads):
+                g = h // per_group
+                next_state[b, h] = (
+                    v_state[b, h] * decay[b : b + 1, h : h + 1]
+                    + upright[h * HEAD_DIM : (h + 1) * HEAD_DIM, b : b + 1]
+                    * keys[b : b + 1, g * STATE : (g + 1) * STATE]
+                )
+
+    update(0, 1)
 
     loads["out"].wait()
     arrive(low_copies)
@@ -367,6 +370,7 @@
     out_squares[t] = gather_rows(low_squares)
     out_copies = exchange("tp", 0, lambda p: out_all.at[t], lambda m: out_all.at[m])
     out_sq_copies = exchange("tp", 1, lambda p: out_squares.at[t], lambda m: out_squares.at[m])
+    update(1, 2)
     arrive(out_sq_copies)
     out_inverse = lax.rsqrt(total(out_squares, tp_count)[:, :1] / INNER + epsilon)
     arrive(out_copies)
@@ -395,6 +399,7 @@
         )
         up_recv[c, z] = up_send[c, z]
     up_sq_recv[z] = up_sq_send[z]
+    update(2, 3)
     arrive(up_sq_copies)
     up_inverse = lax.rsqrt(total(up_sq_recv, kv_count)[:, :1] / D + epsilon)
     act_copies = []
@@ -418,6 +423,7 @@
         down = down + product(acts, v_down[c * chunk : (c + 1) * chunk])
     down_all[t] = down.astype(BF16)
     down_copies = exchange("tp", 2, lambda p: down_all.at[t], lambda m: down_all.at[m])
+    update(3, 4)
     arrive(down_copies)
     layer_out[...] = (residual + total(down_all, tp_count)).astype(BF16)
     for copy in started:

time: 34 us -> 34.1 us (level)
  no operation moved by 1% of the time
where the time goes in v3:
time: 34.1 us; the launch traced here: 33.9 us
  Pallas kernels  31.4 us (92%)
  local copies, waits for them, and re-layouts  1.94 us (6%)
  between operations  0.65 us (2%)
    pallas_call x1, Pallas kernels, per_device(): pl.pallas_call(functools.partial(kernel, kv_count, tp_count), out_shape=(...  31.4 us
    unnamed x2, local copies, waits for them, and re-layouts  1.94 us

profile of v3, /device:TPU:0, one launch (start us, length us, event | category | flops | bytes accessed | tf_op | source)
XLA Modules:
  0.0 33.9 jit_solution(5778834230164331346)
XLA Ops:
  0.6 31.4 %shard_map.203 = (bf16[16,1024]{1,0:T(8,128)(2,1)S(1)}, f32[4,16,64,128]{3,2,1,0:T(8,128)S(1)}) custom-call(bf16[16,1024]{1,0:T(8,128)(2,1)} %h_tokens.1, s32[4]{0:T(128)} %h_lengths.1, bf16[3,4,1024]{2,1,0:T(4,128)(2,1)} %bitcast.3, bf16[4,3,2,256]{3,2,1,0:T(2,128)(2,1)} %h_conv_state_bc.1, bf16[1024]{0:T(1024)(128)(2,1)} %h_norm_gain.1, ...), custom_call_target="tpu_custom_call" | custom-call | tf_op jit(solution)/shard_map/pallas_call | solution.py:469
  32.0 0.6 %copy.24 = bf16[16,1024]{1,0:T(8,128)(2,1)} copy(bf16[16,1024]{1,0:T(8,128)(2,1)S(1)} %get-tuple-element.2) | data formatting | bytes 65536
  32.6 1.3 %copy.25 = f32[4,16,64,128]{3,2,1,0:T(8,128)} copy(f32[4,16,64,128]{3,2,1,0:T(8,128)S(1)} %get-tuple-element.3) | data formatting | bytes 4194304
